TPU v7x, 256 devices: a whole 4x4x8 slice. The times are simulated.
256 devices in a mesh: sp: 16 (over y, x), tp: 16 (over z, core).
Axes of the slice: x: 4, y: 4, z: 8, core: 2. Of those that a mesh axis runs over, the one named last changes fastest.
Arguments:
- query_vectors: bfloat16 [16384, 16, 128], P('sp', 'tp'), may hold values from -6 to 6
- key_vectors: bfloat16 [16384, 16, 128], P('sp', 'tp'), may hold values from -6 to 6
- value_vectors: bfloat16 [16384, 16, 128], P('sp', 'tp'), may hold values from -6 to 6
- out_gate: bfloat16 [16384, 16, 128], P('sp', 'tp'), may hold values from -6 to 6
- decay_rate: float32 [2, 16], P(None, 'tp'), may hold values from 0 to 1
- decay_pre: float32 [2, 16, 16384], P(None, 'tp', 'sp'), may hold values from -6 to 6
- decay_shock: float32 [2, 16, 16384], P(None, 'tp', 'sp'), may hold values from -2 to 0
- beta_pre: float32 [2, 16, 16384], P(None, 'tp', 'sp'), may hold values from -12 to 0
- head_gain: float32 [128], replicated, may hold values from 0.1 to 1.9
- w_out: bfloat16 [2048, 2048], P('tp'), may hold values from -0.125 to 0.125
- tokens: bfloat16 [16384, 2048], P(('sp', 'tp')), may hold values from -6 to 6
- norm_gain: float32 [2048], replicated, may hold values from 0.1 to 1.9
- experts_pick: int32 [16384, 2], P(('sp', 'tp')), may hold values from 0 to 15, as said below
- pair_logits: float32 [16384, 2], P(('sp', 'tp')), may hold values from -6 to 6
- group_logits: float32 [16384, 8], P(('sp', 'tp')), may hold values from -6 to 6
- expert_gate: bfloat16 [16, 2048, 2048], P('sp', None, 'tp'), may hold values from -0.125 to 0.125
- expert_up: bfloat16 [16, 2048, 2048], P('sp', None, 'tp'), may hold values from -0.125 to 0.125
- expert_down: bfloat16 [16, 2048, 2048], P('sp', None, 'tp'), may hold values from -0.5 to 0.5
Outputs:
- layer_out: bfloat16 [16384, 2048], P(('sp', 'tp'))
Inputs may be any that keep to these rules, and one draw needn't show every extreme that they name: `experts_pick`: each token names two different experts of one group of 2 consecutive experts. The 64 tokens of one device fall 8 into each group. At most 8 tokens of one device name any one expert, and in every draw every expert is named by 8 tokens of every device.
All inputs are finite; a program needn't handle non-finite values.
Results may differ from a plain program's by a relative error of at most 0.02.
Values may be sent and summed in bfloat16 or wider, within the bound.
No kernel may reach another device: no remote copies, remote signals or barrier semaphores. Data moves between devices by JAX's collectives and lax.ppermute only.
A program may use at most 128 MiB of HBM per device.

v0:
```python
import jax
import jax.numpy as jnp
from jax import lax
from jax.sharding import Mesh
from jax.sharding import PartitionSpec as P

BLOCK = 64
GROUP_SIZE = 2
SP = ("sp_0", "sp_1")
SP_TP = ("sp_0", "sp_1", "tp")
NORM_EPSILON = 1e-06


def neutral_like(x, identity):
    return jax.tree.map(
        lambda part, zero: jnp.zeros_like(part) + jnp.asarray(zero, part.dtype), x, identity
    )


def prefix_by_axis(x, axes, combine, identity, reverse):
    before = start = neutral_like(x, identity)
    subtotal = x
    for axis in reversed(axes):
        peers, position = (lax.axis_size(axis), lax.axis_index(axis))
        pieces = jax.tree.map(
            lambda part, kind: lax.all_gather(part.astype(kind), axis),
            subtotal,
            (jnp.bfloat16, jnp.bfloat16),
        )
        inside, subtotal = (start, start)
        for k in reversed(range(peers)) if reverse else range(peers):
            passed = k > position if reverse else k < position
            subtotal = combine(
                subtotal, jax.tree.map(lambda part, own: part[k].astype(own.dtype), pieces, x)
            )
            inside = jax.tree.map(lambda new, old: jnp.where(passed, new, old), subtotal, inside)
        before = combine(inside, before)
    return before


def unit_rows(vectors):
    return vectors * lax.rsqrt(jnp.sum(vectors * vectors, axis=-1, keepdims=True) + NORM_EPSILON)


def block_sweep(queries, key_rows, value_rows, log_decay, beta_rate, start_state):
    length, value_width = value_rows.shape
    blocks = length // BLOCK
    query_blocks = queries.reshape(blocks, BLOCK, queries.shape[1])
    key_blocks = key_rows.reshape(blocks, BLOCK, key_rows.shape[1])
    value_blocks = value_rows.reshape(blocks, BLOCK, value_width)
    cumulative = jnp.cumsum(log_decay.reshape(blocks, BLOCK), axis=1)
    beta_blocks = beta_rate.reshape(blocks, BLOCK)
    position = jnp.arange(BLOCK)
    lower_mask = position[:, None] >= position[None, :]
    strict = position[:, None] > position[None, :]
    spread = cumulative[:, :, None] - cumulative[:, None, :]
    within = jnp.where(lower_mask, jnp.exp(jnp.where(lower_mask, spread, 0.0)), 0.0)
    scaled_keys = key_blocks * beta_blocks[:, :, None]
    lower_matrix = jnp.where(
        strict, jnp.einsum("nid,njd->nij", scaled_keys, key_blocks) * within, 0.0
    )
    identity = jnp.eye(BLOCK, dtype=jnp.float32)
    right_side = jnp.concatenate(
        [value_blocks * beta_blocks[:, :, None], scaled_keys * jnp.exp(cumulative)[:, :, None]],
        axis=2,
    )
    solved = jax.scipy.linalg.solve_triangular(
        lower_matrix + identity, right_side, lower=True, unit_diagonal=True
    )
    fresh_values = solved[:, :, :value_width]
    corrections = solved[:, :, value_width:]
    scores = jnp.einsum("nid,njd->nij", query_blocks, key_blocks) * within
    query_decayed = query_blocks * jnp.exp(cumulative)[:, :, None]
    block_total = cumulative[:, -1]
    decayed_keys = key_blocks * jnp.exp(block_total[:, None] - cumulative)[:, :, None]

    def advance(carried, inputs):
        values_in, fix_rows, query_in, key_in, score_in, total_in = inputs
        updated = values_in - jnp.dot(fix_rows, carried)
        output = jnp.dot(query_in, carried) + jnp.dot(score_in, updated)
        carried = carried * jnp.exp(total_in) + jnp.dot(key_in.T, updated)
        return (carried, output)

    final_state, outputs = lax.scan(
        advance,
        start_state,
        (fresh_values, corrections, query_decayed, decayed_keys, scores, block_total),
    )
    return (outputs.reshape(length, value_width), final_state)


def shards(
    query_vectors,
    key_vectors,
    value_vectors,
    out_gate,
    decay_rate,
    decay_pre,
    decay_shock,
    beta_pre,
    head_gain,
    w_out,
    tokens,
    norm_gain,
    experts_pick,
    pair_logits,
    group_logits,
    expert_gate,
    expert_up,
    expert_down,
):
    per_head_width = query_vectors.shape[2]
    queries = unit_rows(
        jnp.transpose(query_vectors.astype(jnp.float32), (1, 0, 2))
    ) * per_head_width ** (-0.5)
    keyset = unit_rows(jnp.transpose(key_vectors.astype(jnp.float32), (1, 0, 2)))
    valueset = jnp.transpose(value_vectors.astype(jnp.float32), (1, 0, 2))
    padded_values = jnp.concatenate([valueset, jnp.zeros_like(keyset)], axis=2)
    log_decay = jnp.moveaxis(
        -decay_rate[:, :, None] * jax.nn.softplus(decay_pre) + decay_shock, 1, 0
    )
    beta_rate = jnp.moveaxis(jax.nn.sigmoid(beta_pre), 1, 0)
    identity = jnp.eye(per_head_width, dtype=jnp.float32)
    opening = jnp.concatenate(
        [jnp.zeros((per_head_width, per_head_width), jnp.float32), identity], axis=1
    )

    def one_head(query_head, key_head, value_head, decay_head, beta_head):
        forward_result, ahead_end = block_sweep(
            query_head, key_head, value_head, decay_head[0], beta_head[0], opening
        )
        trailing_part, behind_end = block_sweep(
            query_head[::-1],
            key_head[::-1],
            value_head[::-1],
            decay_head[1, ::-1],
            beta_head[1, ::-1],
            opening,
        )
        return (forward_result, trailing_part[::-1], ahead_end, behind_end)

    forward_result, trailing_part, ahead_end, behind_end = jax.vmap(one_head)(
        queries, keyset, padded_values, log_decay, beta_rate
    )
    forward_shift = ahead_end[:, :, per_head_width:]
    forward_add = ahead_end[:, :, :per_head_width]
    backward_shift = behind_end[:, :, per_head_width:]
    backward_add = behind_end[:, :, :per_head_width]

    def compose(earlier, later):
        return (
            jnp.einsum("hij,hjk->hik", later[0], earlier[0]),
            jnp.einsum("hij,hjv->hiv", later[0], earlier[1]) + later[1],
        )

    neutral = (jnp.broadcast_to(identity, forward_shift.shape), jnp.zeros_like(forward_add))
    forward_carried = prefix_by_axis((forward_shift, forward_add), SP, compose, neutral, False)[1]
    backward_carried = prefix_by_axis((backward_shift, backward_add), SP, compose, neutral, True)[1]
    joined = (
        forward_result[:, :, :per_head_width]
        + trailing_part[:, :, :per_head_width]
        + jnp.einsum("qfc,qcj->qfj", forward_result[:, :, per_head_width:], forward_carried)
        + jnp.einsum("qfc,qcj->qfj", trailing_part[:, :, per_head_width:], backward_carried)
    )
    joined = jnp.transpose(joined, (1, 0, 2))
    head_scale = lax.rsqrt(jnp.mean(joined * joined, axis=-1, keepdims=True) + NORM_EPSILON)
    mixed_heads = (
        joined * head_scale * head_gain * jax.nn.silu(out_gate.astype(jnp.float32))
    ).astype(jnp.bfloat16)
    mixed_heads = mixed_heads.reshape(joined.shape[0], joined.shape[1] * per_head_width)
    local_rows = tokens.shape[0]
    part_sum = jnp.dot(mixed_heads, w_out, preferred_element_type=jnp.float32).astype(jnp.bfloat16)
    branch_sum = lax.psum_scatter(
        lax.optimization_barrier(part_sum).astype(jnp.float32).astype(jnp.bfloat16),
        "tp",
        scatter_dimension=0,
        tiled=True,
    ).astype(jnp.float32)
    residual = tokens.astype(jnp.float32) + branch_sum
    normed = (
        residual
        * lax.rsqrt(jnp.mean(residual * residual, axis=-1, keepdims=True) + NORM_EPSILON)
        * norm_gain
    ).astype(jnp.bfloat16)
    group_count = group_logits.shape[1]
    group_exp = jnp.exp(group_logits)
    group_share = group_exp / jnp.sum(group_exp, axis=-1, keepdims=True)
    group_index_of = experts_pick[:, 0] // GROUP_SIZE
    group_weight = jnp.sum(
        jnp.where(jnp.arange(group_count)[None, :] == group_index_of[:, None], group_share, 0.0),
        axis=1,
    )
    pair_exp = jnp.exp(pair_logits)
    route_weight = pair_exp / jnp.sum(pair_exp, axis=-1, keepdims=True) * group_weight[:, None]
    capacity = local_rows // group_count
    expert_count = lax.axis_size(SP)
    expert_marks = jnp.sum(
        (
            experts_pick[:, :, None] == jnp.arange(expert_count, dtype=jnp.int32)[None, None, :]
        ).astype(jnp.int32),
        axis=1,
    )
    earlier = jnp.cumsum(expert_marks, axis=0) - expert_marks
    slot_place = experts_pick * capacity + jnp.take_along_axis(earlier, experts_pick, axis=1)
    slot_index = jnp.arange(expert_count * capacity, dtype=jnp.int32)[:, None]
    chooser = (
        (slot_index == slot_place[None, :, 0]) | (slot_index == slot_place[None, :, 1])
    ).astype(jnp.bfloat16)
    outgoing = jnp.dot(chooser, normed, preferred_element_type=jnp.float32).astype(jnp.bfloat16)
    outgoing = outgoing.reshape(expert_count, capacity, normed.shape[1])
    arrived = lax.all_to_all(outgoing, SP, split_axis=0, concat_axis=0, tiled=True)
    source_count, slot_count, model_width = arrived.shape
    row_count = source_count * slot_count
    flat_rows = arrived.reshape(row_count, model_width)
    part_rows = lax.all_gather(flat_rows, "tp", axis=0, tiled=True)
    gate_out = jnp.dot(part_rows, expert_gate[0], preferred_element_type=jnp.float32)
    up_out = jnp.dot(part_rows, expert_up[0], preferred_element_type=jnp.float32)
    hidden = (jax.nn.silu(gate_out) * up_out).astype(jnp.bfloat16)
    product = lax.dot_general(
        hidden, expert_down[0], (((1,), (1,)), ((), ())), preferred_element_type=jnp.float32
    ).astype(jnp.bfloat16)
    summed_out = lax.psum_scatter(
        lax.optimization_barrier(product).astype(jnp.float32).astype(jnp.bfloat16),
        "tp",
        scatter_dimension=0,
        tiled=True,
    )
    expert_rows = summed_out.reshape(source_count, slot_count, model_width)
    results = lax.all_to_all(expert_rows, SP, split_axis=0, concat_axis=0, tiled=True)
    gathered = results.reshape(expert_count * capacity, normed.shape[1])
    chosen = gathered[slot_place]
    mixture = jnp.einsum("tk,tkd->td", route_weight, chosen.astype(jnp.float32))
    return (residual + mixture).astype(jnp.bfloat16)


def solution(mesh):
    finer = Mesh(mesh.devices.reshape(4, 4, mesh.shape["tp"]), ("sp_0", "sp_1", "tp"))
    in_specs = (
        P(SP, "tp", None),
        P(SP, "tp", None),
        P(SP, "tp", None),
        P(SP, "tp", None),
        P(None, "tp"),
        P(None, "tp", SP),
        P(None, "tp", SP),
        P(None, "tp", SP),
        P(),
        P("tp", None),
        P(SP_TP, None),
        P(),
        P(SP_TP, None),
        P(SP_TP, None),
        P(SP_TP, None),
        P(SP, None, "tp"),
        P(SP, None, "tp"),
        P(SP, None, "tp"),
    )
    out_specs = P(SP_TP, None)
    return jax.shard_map(
        shards, mesh=finer, in_specs=in_specs, out_specs=out_specs, check_vma=False
    )
```

profile of v0, /device:TPU:2, one launch (start us, length us, event | category | flops | bytes accessed | tf_op | source)
XLA Modules:
  0.0 675.1 jit_solution(16698587801744514501)
XLA Ops:
  6.5 1.2 fusion.92
  7.8 1.0 convert_element_type.213
  12.5 78.6 %custom-call.6 = f32[1,16,1,64,64]{3,4,2,1,0:T(8,128)S(1)} custom-call(f32[1,16,1,64,64]{4,3,2,1,0:T(8,128)S(1)} %fusion.59), custom_call_target="InvertDiagBlocksLowerTriangular" | custom-call | tf_op jit(solution)/shard_map/vmap(jit(_solve_triangular))/vmap()/triangular_solve | solution.py:67
  92.1 1.5 fusion.45
  93.6 1.1 slice_bitcast_fusion.1
  96.5 1.0 bitcast_multiply_fusion.2
  101.2 3.4 rev.17
  105.1 2.0 fusion.62
  107.1 79.4 %custom-call.7 = f32[1,16,1,64,64]{3,4,2,1,0:T(8,128)S(1)} custom-call(f32[1,16,1,64,64]{4,3,2,1,0:T(8,128)} %fusion.62), custom_call_target="InvertDiagBlocksLowerTriangular" | custom-call | tf_op jit(solution)/shard_map/vmap(jit(_solve_triangular))/vmap()/triangular_solve | solution.py:67
  187.1 1.5 fusion.44
  188.6 1.1 slice_bitcast_fusion
  192.6 53.2 %while.25 = (s32[]{:T(128)}, f32[1,128,256]{2,1,0:T(8,128)S(1)}, f32[16,1,64,256]{3,2,1,0:T(8,128)S(1)}, f32[16,1]{0,1:T(1,128)S(1)}, bf16[16,1,64,128]{3,2,1,0:...) while((s32[]{:T(128)}, f32[1,128,256]{2,1,0:T(8,128)S(1)}, ...), condition=%wide.region_7.9_spmd, body=%wide.region_6.8_spmd.sunk | while | flops 14794754 | bytes 952445 | solution.py:84
  195.9 1.0 convolution_subtract_fusion.5
  199.2 1.0 convolution_subtract_fusion.5
  202.6 1.0 convolution_subtract_fusion.5
  205.9 1.0 convolution_subtract_fusion.5
  209.2 1.0 convolution_subtract_fusion.5
  212.6 1.0 convolution_subtract_fusion.5
  215.9 1.0 convolution_subtract_fusion.5
  219.2 1.0 convolution_subtract_fusion.5
  222.5 1.0 convolution_subtract_fusion.5
  225.9 1.0 convolution_subtract_fusion.5
  229.2 1.0 convolution_subtract_fusion.5
  232.5 1.0 convolution_subtract_fusion.5
  235.9 1.0 convolution_subtract_fusion.5
  239.2 1.0 convolution_subtract_fusion.5
  242.5 1.0 convolution_subtract_fusion.5
  246.9 1.2 fusion.50
  248.9 54.2 %while.24 = (s32[]{:T(128)}, f32[1,128,256]{2,1,0:T(8,128)S(1)}, f32[16,1,64,256]{3,2,1,0:T(8,128)S(1)}, f32[16,1]{0,1:T(1,128)S(1)}, bf16[16,1,64,128]{3,2,1,0:...) while((s32[]{:T(128)}, f32[1,128,256]{2,1,0:T(8,128)S(1)}, ...), condition=%wide.region_4.6_spmd, body=%wide.region_3.5_spmd.sunk | while | flops 14794754 | bytes 952445 | solution.py:84
  248.9 1.0 convolution_subtract_fusion.4
  252.3 1.0 convolution_subtract_fusion.4
  255.7 1.0 convolution_subtract_fusion.4
  259.0 1.0 convolution_subtract_fusion.4
  262.4 1.0 convolution_subtract_fusion.4
  265.8 1.0 convolution_subtract_fusion.4
  269.2 1.0 convolution_subtract_fusion.4
  286.1 1.0 convolution_subtract_fusion.4
  303.1 12.1 %all-gather = bf16[4,128,128]{2,1,0:T(8,128)(2,1)S(1)} all-gather(bf16[1,128,128]{2,1,0:T(8,128)(2,1)S(1)} %get-tuple-element.234), channel_id=2, replica_groups=mesh['sp_0'=4,'sp_1'=4,'tp'=16] {'sp_1'}, dimensions={0}, use_global_device_ids=true | all-gather | bytes 163840 | tf_op jit(solution)/shard_map/all_gather | solution.py:26
  316.3 12.5 %all-gather.1 = bf16[512,128]{1,0:T(8,128)(2,1)S(1)} all-gather(bf16[128,128]{1,0:T(8,128)(2,1)S(1)} %fusion.226), channel_id=3, replica_groups=mesh['sp_0'=4,'sp_1'=4,'tp'=16] {'sp_0'}, dimensions={0}, use_global_device_ids=true | all-gather | bytes 163840 | tf_op jit(solution)/shard_map/all_gather | solution.py:26
  328.8 12.0 %all-gather.2 = bf16[4,128,128]{2,1,0:T(8,128)(2,1)S(1)} all-gather(bf16[1,128,128]{2,1,0:T(8,128)(2,1)S(1)} %get-tuple-element.235), channel_id=4, replica_groups=mesh['sp_0'=4,'sp_1'=4,'tp'=16] {'sp_1'}, dimensions={0}, use_global_device_ids=true | all-gather | bytes 163840 | tf_op jit(solution)/shard_map/all_gather | solution.py:26
  342.0 12.0 %all-gather.3 = bf16[512,128]{1,0:T(8,128)(2,1)S(1)} all-gather(bf16[128,128]{1,0:T(8,128)(2,1)S(1)} %convolution_add_fusion.15), channel_id=5, replica_groups=mesh['sp_0'=4,'sp_1'=4,'tp'=16] {'sp_0'}, dimensions={0}, use_global_device_ids=true | all-gather | bytes 163840 | tf_op jit(solution)/shard_map/all_gather | solution.py:26
  355.1 12.0 %all-gather.4 = bf16[4,128,128]{2,1,0:T(8,128)(2,1)S(1)} all-gather(bf16[1,128,128]{2,1,0:T(8,128)(2,1)S(1)} %get-tuple-element.236), channel_id=6, replica_groups=mesh['sp_0'=4,'sp_1'=4,'tp'=16] {'sp_1'}, dimensions={0}, use_global_device_ids=true | all-gather | bytes 163840 | tf_op jit(solution)/shard_map/all_gather | solution.py:26
  368.7 12.2 %all-gather.5 = bf16[512,128]{1,0:T(8,128)(2,1)S(1)} all-gather(bf16[128,128]{1,0:T(8,128)(2,1)S(1)} %fusion.229), channel_id=7, replica_groups=mesh['sp_0'=4,'sp_1'=4,'tp'=16] {'sp_0'}, dimensions={0}, use_global_device_ids=true | all-gather | bytes 163840 | tf_op jit(solution)/shard_map/all_gather | solution.py:26
  380.9 12.0 %all-gather.6 = bf16[4,128,128]{2,1,0:T(8,128)(2,1)S(1)} all-gather(bf16[1,128,128]{2,1,0:T(8,128)(2,1)S(1)} %get-tuple-element.237), channel_id=8, replica_groups=mesh['sp_0'=4,'sp_1'=4,'tp'=16] {'sp_1'}, dimensions={0}, use_global_device_ids=true | all-gather | bytes 163840 | tf_op jit(solution)/shard_map/all_gather | solution.py:26
  394.5 12.0 %all-gather.7 = bf16[512,128]{1,0:T(8,128)(2,1)S(1)} all-gather(bf16[128,128]{1,0:T(8,128)(2,1)S(1)} %convolution_add_fusion.6), channel_id=9, replica_groups=mesh['sp_0'=4,'sp_1'=4,'tp'=16] {'sp_0'}, dimensions={0}, use_global_device_ids=true | all-gather | bytes 163840 | tf_op jit(solution)/shard_map/all_gather | solution.py:26
  409.1 1.0 copy.130
  410.1 3.9 slice.185
  414.0 1.2 fusion.64
  415.2 2.0 convolution_bitcast_fusion.2
  417.3 1.7 fusion.68
  419.0 1.5 multiply_reduce_fusion.1
  420.5 1.1 copy.119
  421.6 4.3 convolution_convert_fusion.1
  427.1 1.3 gather_fusion.1
  428.6 61.8 %reduce-scatter.3.cloned.1.call-done = bf16[64,2048]{1,0:T(8,128)(2,1)} async-done(((bf16[1024,2048]{1,0:T(8,128)(2,1)}), bf16[64,2048]{1,0:T(8,128)(2,1)}) %reduce-scatter.3.cloned.1.call-update) | async-done | bytes 262160 | tf_op jit(solution)/shard_map/reduce_scatter | solution.py:173
  490.5 1.1 multiply_reduce_fusion
  491.6 1.3 fusion.37
  493.0 16.0 %all_to_all.10 = bf16[16,8,2048]{2,1,0:T(8,128)(2,1)} all-to-all(bf16[16,8,2048]{2,1,0:T(8,128)(2,1)S(1)} %fusion.37), channel_id=1, replica_groups=mesh['sp_0'=4,'sp_1'=4,'tp'=16] {'sp_0','sp_1'}, dimensions={0} | all-to-all | bytes 1048576 | tf_op jit(solution)/shard_map/all_to_all | solution.py:211
  509.0 52.6 %all-gather.10.cloned.1.call-done = bf16[2048,2048]{1,0:T(8,128)(2,1)} async-done(((bf16[128,2048]{1,0:T(8,128)(2,1)}), bf16[2048,2048]{1,0:T(8,128)(2,1)}) %all-gather.10.cloned.1.call-update) | async-done | bytes 8388624 | tf_op jit(solution)/shard_map/all_gather | solution.py:215
  561.6 5.7 fusion.86
  567.3 12.8 %convolution_convert_fusion = bf16[2048,2048]{1,0:T(8,128)(2,1)} fusion(bf16[2048,2048]{1,0:T(8,128)(2,1)} %all-gather.10.cloned.1.call-done, f32[2048,128]{1,0:T(8,128)S(1)} %fusion.86, bf16[1,2048,128]{2,1,0:T(8,128)(2,1)S(1)} %copy-done, bf16[1,2048,128]{2,1,0:T(8,128)(2,1)S(1)} %copy-done.6), kind=kOutput, calls=%fused_computation.46 | convolution fusion | flops 2153250816 | bytes 18874368 | tf_op jit(solution)/shard_map/dot_general | solution.py:219
  580.9 68.7 %reduce-scatter.5.cloned.1.call-done = bf16[128,2048]{1,0:T(8,128)(2,1)} async-done(((bf16[2048,2048]{1,0:T(8,128)(2,1)}), bf16[128,2048]{1,0:T(8,128)(2,1)}) %reduce-scatter.5.cloned.1.call-update) | async-done | bytes 524304 | tf_op jit(solution)/shard_map/reduce_scatter | solution.py:222
  649.6 7.3 %all-to-all-start.1 = ((bf16[16,8,2048]{2,1,0:T(8,128)(2,1)}), bf16[16,8,2048]{2,1,0:T(8,128)(2,1)S(1)}, u32[]{:S(2)}, u32[]{:S(2)}) async-start(bf16[16,8,2048]{2,1,0:T(8,128)(2,1)} %bitcast.435), calls=%async_computation.3 | async-start | bytes 1048576 | tf_op jit(solution)/shard_map/all_to_all | solution.py:229
  657.3 8.3 %all-to-all-done.1 = bf16[16,8,2048]{2,1,0:T(8,128)(2,1)S(1)} async-done(((bf16[16,8,2048]{2,1,0:T(8,128)(2,1)}), bf16[16,8,2048]{2,1,0:T(8,128)(2,1)S(1)}, u32[]{:S(2)}, u32[]{:S(2)}) %all-to-all-start.1) | async-done | bytes 524320 | tf_op jit(solution)/shard_map/all_to_all | solution.py:229
  (365 shorter events, 114.0 us)
Async XLA Ops:
  6.5 560.8 %copy-start = (bf16[1,2048,128]{2,1,0:T(8,128)(2,1)S(1)}, bf16[1,2048,128]{2,1,0:T(8,128)(2,1)}, u32[]{:S(2)}) copy-start(bf16[1,2048,128]{2,1,0:T(8,128)(2,1)} %param.41) | copy-start | bytes 1572868
  6.5 483.9 %reduce-scatter.3.cloned.1.call-start = ((), (), s32[]{:S(2)}) async-start(), calls=%async_computation.4 | async-start | bytes 4456448 | tf_op jit(solution)/shard_map/reduce_scatter | solution.py:173
  7.8 83.5 %copy-start.22 = (bf16[1024,1,128]{2,0,1:T(8,128)(2,1)S(1)}, bf16[1024,1,128]{2,0,1:T(8,128)(2,1)}, u32[]{:S(2)}) copy-start(bf16[1024,1,128]{2,0,1:T(8,128)(2,1)} %param.26) | copy-start | bytes 786436
  8.8 82.5 %copy-start.41 = (f32[64,64]{1,0:T(8,128)}, f32[64,64]{1,0:T(8,128)S(1)}, u32[]{:S(2)}) copy-start(f32[64,64]{1,0:T(8,128)S(1)} %get-tuple-element.256) | copy-start | bytes 49156
  8.8 82.5 %copy-start.47 = (pred[64,64]{1,0:T(8,128)(4,1)}, pred[64,64]{1,0:T(8,128)(4,1)S(1)}, u32[]{:S(2)}) copy-start(pred[64,64]{1,0:T(8,128)(4,1)S(1)} %get-tuple-element.255) | copy-start | bytes 12292
  8.9 82.5 %copy-start.42 = (f32[64,64]{1,0:T(8,128)}, f32[64,64]{1,0:T(8,128)S(1)}, u32[]{:S(2)}) copy-start(f32[64,64]{1,0:T(8,128)S(1)} %fusion.185) | copy-start | bytes 49156
  11.3 80.0 %copy-start.49 = (pred[64,64]{1,0:T(8,128)(4,1)}, pred[64,64]{1,0:T(8,128)(4,1)S(1)}, u32[]{:S(2)}) copy-start(pred[64,64]{1,0:T(8,128)(4,1)S(1)} %get-tuple-element.253) | copy-start | bytes 12292
  11.8 79.6 %copy-start.51 = (f32[16]{0:T(128)}, f32[16]{0:T(128)S(1)}, u32[]{:S(2)}) copy-start(f32[16]{0:T(128)S(1)} %slice_reduce_fusion.1) | copy-start | bytes 196
  93.6 1.9 copy-start.4
  93.6 2.9 copy-start.3
  97.5 7.5 %copy-start.48 = (pred[64,64]{1,0:T(8,128)(4,1)S(1)}, pred[64,64]{1,0:T(8,128)(4,1)}, u32[]{:S(2)}) copy-start(pred[64,64]{1,0:T(8,128)(4,1)} %copy-done.47) | copy-start | bytes 12292
  105.1 81.7 %copy-start.53 = (f32[16]{0:T(128)}, f32[16]{0:T(128)S(1)}, u32[]{:S(2)}) copy-start(f32[16]{0:T(128)S(1)} %slice_reduce_fusion) | copy-start | bytes 196
  192.0 0.6 copy-start.54
  245.8 1.0 copy-start.5
  248.1 0.8 copy-start.52
  315.3 0.6 copy-start.32
  316.0 12.8 %copy-start.23 = (bf16[128,128]{1,0:T(8,128)(2,1)}, bf16[128,128]{1,0:T(8,128)(2,1)S(1)}, u32[]{:S(2)}) copy-start(bf16[128,128]{1,0:T(8,128)(2,1)S(1)} %fusion.228) | copy-start | bytes 98308
  316.2 12.7 %copy-start.25 = (bf16[128,128]{1,0:T(8,128)(2,1)}, bf16[128,128]{1,0:T(8,128)(2,1)S(1)}, u32[]{:S(2)}) copy-start(bf16[128,128]{1,0:T(8,128)(2,1)S(1)} %fusion.227) | copy-start | bytes 98308
  316.3 12.5 %copy-start.27 = (bf16[128,128]{1,0:T(8,128)(2,1)}, bf16[128,128]{1,0:T(8,128)(2,1)S(1)}, u32[]{:S(2)}) copy-start(bf16[128,128]{1,0:T(8,128)(2,1)S(1)} %fusion.226) | copy-start | bytes 98308
  341.0 27.1 %copy-start.10 = (bf16[128,128]{1,0:T(8,128)(2,1)}, bf16[128,128]{1,0:T(8,128)(2,1)S(1)}, u32[]{:S(2)}) copy-start(bf16[128,128]{1,0:T(8,128)(2,1)S(1)} %convolution_add_fusion.18) | copy-start | bytes 98308
  341.1 0.6 copy-start.14
  341.8 26.2 %copy-start.16 = (bf16[128,128]{1,0:T(8,128)(2,1)}, bf16[128,128]{1,0:T(8,128)(2,1)S(1)}, u32[]{:S(2)}) copy-start(bf16[128,128]{1,0:T(8,128)(2,1)S(1)} %convolution_add_fusion.16) | copy-start | bytes 98308
  342.0 26.1 %copy-start.12 = (bf16[128,128]{1,0:T(8,128)(2,1)}, bf16[128,128]{1,0:T(8,128)(2,1)S(1)}, u32[]{:S(2)}) copy-start(bf16[128,128]{1,0:T(8,128)(2,1)S(1)} %convolution_add_fusion.15) | copy-start | bytes 98308
  354.0 52.7 %copy-start.7 = (bf16[512,128]{1,0:T(8,128)(2,1)}, bf16[512,128]{1,0:T(8,128)(2,1)S(1)}, u32[]{:S(2)}) copy-start(bf16[512,128]{1,0:T(8,128)(2,1)S(1)} %all-gather.3) | copy-start | bytes 393220
  354.1 0.9 copy-start.35
  354.3 0.8 copy-start.38
  367.2 0.6 copy-start.34
  367.9 0.6 copy-start.29
  368.5 12.3 %copy-start.30 = (bf16[128,128]{1,0:T(8,128)(2,1)}, bf16[128,128]{1,0:T(8,128)(2,1)S(1)}, u32[]{:S(2)}) copy-start(bf16[128,128]{1,0:T(8,128)(2,1)S(1)} %fusion.230) | copy-start | bytes 98308
  368.7 24.2 %copy-start.31 = (bf16[128,128]{1,0:T(8,128)(2,1)}, bf16[128,128]{1,0:T(8,128)(2,1)S(1)}, u32[]{:S(2)}) copy-start(bf16[128,128]{1,0:T(8,128)(2,1)S(1)} %fusion.229) | copy-start | bytes 98308
  380.8 27.9 %copy-start.8 = (bf16[512,128]{1,0:T(8,128)(2,1)}, bf16[512,128]{1,0:T(8,128)(2,1)S(1)}, u32[]{:S(2)}) copy-start(bf16[512,128]{1,0:T(8,128)(2,1)S(1)} %all-gather.5) | copy-start | bytes 393220
  393.0 0.6 copy-start.18
  393.1 0.6 copy-start.20
  393.7 0.6 copy-start.21
  394.4 12.3 %copy-start.19 = (bf16[128,128]{1,0:T(8,128)(2,1)}, bf16[128,128]{1,0:T(8,128)(2,1)S(1)}, u32[]{:S(2)}) copy-start(bf16[128,128]{1,0:T(8,128)(2,1)S(1)} %convolution_add_fusion.6) | copy-start | bytes 98308
  406.5 2.3 copy-start.9
  406.6 0.6 copy-start.37
  407.2 0.6 copy-start.40
  410.1 7.2 %copy-start.24 = (bf16[128,128]{1,0:T(8,128)(2,1)S(1)}, bf16[128,128]{1,0:T(8,128)(2,1)}, u32[]{:S(2)}) copy-start(bf16[128,128]{1,0:T(8,128)(2,1)} %copy-done.23) | copy-start | bytes 98308
  410.1 7.2 %copy-start.26 = (bf16[128,128]{1,0:T(8,128)(2,1)S(1)}, bf16[128,128]{1,0:T(8,128)(2,1)}, u32[]{:S(2)}) copy-start(bf16[128,128]{1,0:T(8,128)(2,1)} %copy-done.25) | copy-start | bytes 98308
  410.1 7.2 %copy-start.28 = (bf16[128,128]{1,0:T(8,128)(2,1)S(1)}, bf16[128,128]{1,0:T(8,128)(2,1)}, u32[]{:S(2)}) copy-start(bf16[128,128]{1,0:T(8,128)(2,1)} %copy-done.27) | copy-start | bytes 98308
  410.1 7.2 %copy-start.33 = (bf16[128,128]{1,0:T(8,128)(2,1)S(1)}, bf16[128,128]{1,0:T(8,128)(2,1)}, u32[]{:S(2)}) copy-start(bf16[128,128]{1,0:T(8,128)(2,1)} %copy-done.32) | copy-start | bytes 98308
  410.1 7.2 %copy-start.36 = (bf16[128,128]{1,0:T(8,128)(2,1)S(1)}, bf16[128,128]{1,0:T(8,128)(2,1)}, u32[]{:S(2)}) copy-start(bf16[128,128]{1,0:T(8,128)(2,1)} %copy-done.35) | copy-start | bytes 98308
  410.1 7.2 %copy-start.39 = (bf16[128,128]{1,0:T(8,128)(2,1)S(1)}, bf16[128,128]{1,0:T(8,128)(2,1)}, u32[]{:S(2)}) copy-start(bf16[128,128]{1,0:T(8,128)(2,1)} %copy-done.38) | copy-start | bytes 98308
  410.1 7.2 %copy-start.43 = (bf16[128,128]{1,0:T(8,128)(2,1)S(1)}, bf16[128,128]{1,0:T(8,128)(2,1)}, u32[]{:S(2)}) copy-start(bf16[128,128]{1,0:T(8,128)(2,1)} %convolution_add_fusion.13) | copy-start | bytes 98308
  410.1 8.8 %copy-start.11 = (bf16[128,128]{1,0:T(8,128)(2,1)S(1)}, bf16[128,128]{1,0:T(8,128)(2,1)}, u32[]{:S(2)}) copy-start(bf16[128,128]{1,0:T(8,128)(2,1)} %copy-done.10) | copy-start | bytes 98308
  410.1 8.8 %copy-start.13 = (bf16[128,128]{1,0:T(8,128)(2,1)S(1)}, bf16[128,128]{1,0:T(8,128)(2,1)}, u32[]{:S(2)}) copy-start(bf16[128,128]{1,0:T(8,128)(2,1)} %copy-done.12) | copy-start | bytes 98308
  410.1 8.8 %copy-start.15 = (bf16[128,128]{1,0:T(8,128)(2,1)S(1)}, bf16[128,128]{1,0:T(8,128)(2,1)}, u32[]{:S(2)}) copy-start(bf16[128,128]{1,0:T(8,128)(2,1)} %copy-done.14) | copy-start | bytes 98308
  410.1 8.8 %copy-start.17 = (bf16[128,128]{1,0:T(8,128)(2,1)S(1)}, bf16[128,128]{1,0:T(8,128)(2,1)}, u32[]{:S(2)}) copy-start(bf16[128,128]{1,0:T(8,128)(2,1)} %copy-done.16) | copy-start | bytes 98308
  419.0 2.6 copy-start.50
  426.0 0.7 copy-start.45
  426.0 135.6 %all-gather.10.cloned.1.call-start = ((), (), s32[]{:S(2)}) async-start(), calls=%async_computation.5 | async-start | bytes 8912896 | tf_op jit(solution)/shard_map/all_gather | solution.py:215
  427.1 63.4 %copy-start.1 = (bf16[64,2048]{1,0:T(8,128)(2,1)S(1)}, bf16[64,2048]{1,0:T(8,128)(2,1)}, u32[]{:S(2)}) copy-start(bf16[64,2048]{1,0:T(8,128)(2,1)} %param.34) | copy-start | bytes 786436
  427.1 64.5 %copy-start.46 = (f32[2048]{0:T(1024)S(1)}, f32[2048]{0:T(1024)}, u32[]{:S(2)}) copy-start(f32[2048]{0:T(1024)} %param.35) | copy-start | bytes 24580
  428.6 133.0 %copy-start.56 = (bf16[1,2048,128]{2,1,0:T(8,128)(2,1)S(1)}, bf16[1,2048,128]{2,1,0:T(8,128)(2,1)}, u32[]{:S(2)}) copy-start(bf16[1,2048,128]{2,1,0:T(8,128)(2,1)} %param.39) | copy-start | bytes 1572868
  508.9 58.4 %copy-start.6 = (bf16[1,2048,128]{2,1,0:T(8,128)(2,1)S(1)}, bf16[1,2048,128]{2,1,0:T(8,128)(2,1)}, u32[]{:S(2)}) copy-start(bf16[1,2048,128]{2,1,0:T(8,128)(2,1)} %param.40) | copy-start | bytes 1572868
  509.0 140.7 %reduce-scatter.5.cloned.1.call-start = ((), (), s32[]{:S(2)}) async-start(), calls=%async_computation.6 | async-start | bytes 8912896 | tf_op jit(solution)/shard_map/reduce_scatter | solution.py:222
  580.2 0.7 copy-start.44
  580.2 76.7 %copy-start.55 = (f32[64,2]{0,1:T(2,128)S(1)}, f32[64,2]{0,1:T(2,128)}, u32[]{:S(2)}) copy-start(f32[64,2]{0,1:T(2,128)} %param.37) | copy-start | bytes 1540
  649.6 16.1 %all-to-all-start.1 = ((bf16[16,8,2048]{2,1,0:T(8,128)(2,1)}), bf16[16,8,2048]{2,1,0:T(8,128)(2,1)S(1)}, u32[]{:S(2)}, u32[]{:S(2)}) async-start(bf16[16,8,2048]{2,1,0:T(8,128)(2,1)} %bitcast.435), calls=%async_computation.3 | async-start | bytes 1048576 | tf_op jit(solution)/shard_map/all_to_all | solution.py:229
  666.6 1.0 copy-start.2
Sparse Core Ops, SparseCore 0:
  426.1 64.3 reduce-scatter.2
  509.1 52.4 all-gather.9
  580.3 69.2 reduce-scatter.4
where the time goes:
time: 682 us; the launch traced here: 675 us
  waiting for transfers between devices  192 us (28%)
  other arithmetic  171 us (25%)
  matrix products  132 us (19%)
  blocking collectives  113 us (17%)
  local copies, waits for them, and re-layouts  46 us (7%)
  between operations  14.1 us (2%)
  starting transfers between devices  7.36 us (1%)
    another operation x5, other arithmetic, block_sweep(): jax.scipy.linalg.solve_triangular(lower_matrix + identity, right_side, lo...  158 us
    all_gather x8, blocking collectives, prefix_by_axis(): lax.all_gather(part.astype(kind), axis)  96.7 us
    reduce_scatter x1, waiting for transfers between devices, shards(): lax.psum_scatter(lax.optimization_barrier(product).astype(jnp.float32).as...  68.7 us
    reduce_scatter x1, waiting for transfers between devices, shards(): lax.psum_scatter(lax.optimization_barrier(part_sum).astype(jnp.float32).a...  61.8 us
    all_gather x1, waiting for transfers between devices, shards(): part_rows = lax.all_gather(flat_rows, 'tp', axis=0, tiled=True)  52.6 us
    dot_general x32, matrix products, advance(): updated = values_in - jnp.dot(fix_rows, carried)  31.8 us
    dot_general x64, matrix products, advance(): output = jnp.dot(query_in, carried) + jnp.dot(score_in, updated)  31.7 us
    dot_general x32, matrix products, advance(): carried = carried * jnp.exp(total_in) + jnp.dot(key_in.T, updated)  24.8 us
  transfers between devices with their start and end apart: 4, of which 4 were waited for; matrix products, arithmetic and copies ran while one was open for 0% of the time, Pallas kernels for 0%

commit v1 on v0

--- a/solution.py
+++ b/solution.py
@@ -212,7 +212,9 @@
     source_count, slot_count, model_width = arrived.shape
     row_count = source_count * slot_count
     flat_rows = arrived.reshape(row_count, model_width)
-    part_rows = lax.all_gather(flat_rows, "tp", axis=0, tiled=True)
+    part_rows = jnp.concatenate(
+        lax.all_to_all(jnp.stack([flat_rows] * lax.axis_size("tp")), "tp", 0, 0), axis=0
+    )
     gate_out = jnp.dot(part_rows, expert_gate[0], preferred_element_type=jnp.float32)
     up_out = jnp.dot(part_rows, expert_up[0], preferred_element_type=jnp.float32)
     hidden = (jax.nn.silu(gate_out) * up_out).astype(jnp.bfloat16)

time: 682 us -> 821 us (1.20)
  blocking collectives: 113 us -> 302 us
  waiting for transfers between devices: 192 us -> 136 us
    all_to_all x0 -> x1, blocking collectives: none -> 190 us  [shards(): lax.all_to_all(jnp.stack([flat_rows] * lax.axis_size('tp')), 'tp', 0, 0)]
    all_gather x1 -> x0, waiting for transfers between devices: 52.6 us -> none  [shards(): part_rows = lax.all_gather(flat_rows, 'tp', axis=0, tiled=True)]
  transfers between devices with their start and end apart: 4 -> 3, of which waited for: 4 -> 3; matrix products, arithmetic and copies ran while one was open for 0% -> 0% of each run, Pallas kernels for 0% -> 0%
where the time goes in v1:
time: 821 us; the launch traced here: 814 us
  blocking collectives  302 us (37%)
  other arithmetic  171 us (21%)
  waiting for transfers between devices  136 us (17%)
  matrix products  130 us (16%)
  local copies, waits for them, and re-layouts  51.8 us (6%)
  between operations  14.4 us (2%)
    all_to_all x1, blocking collectives, shards(): lax.all_to_all(jnp.stack([flat_rows] * lax.axis_size('tp')), 'tp', 0, 0)  190 us
    another operation x5, other arithmetic, block_sweep(): jax.scipy.linalg.solve_triangular(lower_matrix + identity, right_side, lo...  158 us
    all_gather x8, blocking collectives, prefix_by_axis(): lax.all_gather(part.astype(kind), axis)  96.7 us
    reduce_scatter x1, waiting for transfers between devices, shards(): lax.psum_scatter(lax.optimization_barrier(product).astype(jnp.float32).as...  65.8 us
    reduce_scatter x1, waiting for transfers between devices, shards(): lax.psum_scatter(lax.optimization_barrier(part_sum).astype(jnp.float32).a...  61.9 us
    dot_general x32, matrix products, advance(): updated = values_in - jnp.dot(fix_rows, carried)  31.8 us
    dot_general x64, matrix products, advance(): output = jnp.dot(query_in, carried) + jnp.dot(score_in, updated)  31.7 us
    dot_general x32, matrix products, advance(): carried = carried * jnp.exp(total_in) + jnp.dot(key_in.T, updated)  27 us
  transfers between devices with their start and end apart: 3, of which 3 were waited for; matrix products, arithmetic and copies ran while one was open for 0% of the time, Pallas kernels for 0%

profile of v1, /device:TPU:2, one launch (start us, length us, event | category | flops | bytes accessed | tf_op | source)
XLA Modules:
  0.0 814.4 jit_solution(12950232169389666617)
XLA Ops:
  6.5 1.2 fusion.92
  7.8 1.0 convert_element_type.213
  12.5 78.6 %custom-call.6 = f32[1,16,1,64,64]{3,4,2,1,0:T(8,128)S(1)} custom-call(f32[1,16,1,64,64]{4,3,2,1,0:T(8,128)S(1)} %fusion.59), custom_call_target="InvertDiagBlocksLowerTriangular" | custom-call | tf_op jit(solution)/shard_map/vmap(jit(_solve_triangular))/vmap()/triangular_solve | solution.py:67
  92.1 1.5 fusion.45
  93.6 1.1 slice_bitcast_fusion.1
  96.5 1.0 bitcast_multiply_fusion.2
  101.5 3.4 rev.17
  105.4 2.0 fusion.62
  107.4 79.4 %custom-call.7 = f32[1,16,1,64,64]{3,4,2,1,0:T(8,128)S(1)} custom-call(f32[1,16,1,64,64]{4,3,2,1,0:T(8,128)} %fusion.62), custom_call_target="InvertDiagBlocksLowerTriangular" | custom-call | tf_op jit(solution)/shard_map/vmap(jit(_solve_triangular))/vmap()/triangular_solve | solution.py:67
  187.4 1.5 fusion.44
  188.9 1.1 slice_bitcast_fusion
  192.9 54.0 %while.25 = (s32[]{:T(128)}, f32[1,128,256]{2,1,0:T(8,128)S(1)}, f32[16,1,64,256]{3,2,1,0:T(8,128)S(1)}, f32[16,1]{0,1:T(1,128)S(1)}, bf16[16,1,64,128]{3,2,1,0:...) while((s32[]{:T(128)}, f32[1,128,256]{2,1,0:T(8,128)S(1)}, ...), condition=%wide.region_7.9_spmd, body=%wide.region_6.8_spmd.sunk | while | flops 14794754 | bytes 952445 | solution.py:84
  196.3 1.0 convolution_subtract_fusion.5
  199.6 1.0 convolution_subtract_fusion.5
  203.0 1.0 convolution_subtract_fusion.5
  206.4 1.0 convolution_subtract_fusion.5
  209.8 1.0 convolution_subtract_fusion.5
  213.2 1.0 convolution_subtract_fusion.5
  216.5 1.0 convolution_subtract_fusion.5
  219.9 1.0 convolution_subtract_fusion.5
  223.3 1.0 convolution_subtract_fusion.5
  226.7 1.0 convolution_subtract_fusion.5
  230.0 1.0 convolution_subtract_fusion.5
  233.4 1.0 convolution_subtract_fusion.5
  236.8 1.0 convolution_subtract_fusion.5
  240.2 1.0 convolution_subtract_fusion.5
  243.5 1.0 convolution_subtract_fusion.5
  248.0 1.2 fusion.50
  250.0 57.1 %while.24 = (s32[]{:T(128)}, f32[1,128,256]{2,1,0:T(8,128)S(1)}, f32[16,1,64,256]{3,2,1,0:T(8,128)S(1)}, f32[16,1]{0,1:T(1,128)S(1)}, bf16[16,1,64,128]{3,2,1,0:...) while((s32[]{:T(128)}, f32[1,128,256]{2,1,0:T(8,128)S(1)}, ...), condition=%wide.region_4.6_spmd, body=%wide.region_3.5_spmd.sunk | while | flops 14794754 | bytes 952445 | solution.py:84
  250.0 1.0 convolution_subtract_fusion.4
  253.5 1.0 convolution_subtract_fusion.4
  257.1 1.0 convolution_subtract_fusion.4
  260.7 1.0 convolution_subtract_fusion.4
  264.2 1.0 convolution_subtract_fusion.4
  267.8 1.0 convolution_subtract_fusion.4
  307.1 12.1 %all-gather = bf16[4,128,128]{2,1,0:T(8,128)(2,1)S(1)} all-gather(bf16[1,128,128]{2,1,0:T(8,128)(2,1)S(1)} %get-tuple-element.234), channel_id=2, replica_groups=mesh['sp_0'=4,'sp_1'=4,'tp'=16] {'sp_1'}, dimensions={0}, use_global_device_ids=true | all-gather | bytes 163840 | tf_op jit(solution)/shard_map/all_gather | solution.py:26
  320.3 12.5 %all-gather.1 = bf16[512,128]{1,0:T(8,128)(2,1)S(1)} all-gather(bf16[128,128]{1,0:T(8,128)(2,1)S(1)} %fusion.226), channel_id=3, replica_groups=mesh['sp_0'=4,'sp_1'=4,'tp'=16] {'sp_0'}, dimensions={0}, use_global_device_ids=true | all-gather | bytes 163840 | tf_op jit(solution)/shard_map/all_gather | solution.py:26
  332.8 12.0 %all-gather.2 = bf16[4,128,128]{2,1,0:T(8,128)(2,1)S(1)} all-gather(bf16[1,128,128]{2,1,0:T(8,128)(2,1)S(1)} %get-tuple-element.235), channel_id=4, replica_groups=mesh['sp_0'=4,'sp_1'=4,'tp'=16] {'sp_1'}, dimensions={0}, use_global_device_ids=true | all-gather | bytes 163840 | tf_op jit(solution)/shard_map/all_gather | solution.py:26
  346.0 12.0 %all-gather.3 = bf16[512,128]{1,0:T(8,128)(2,1)S(1)} all-gather(bf16[128,128]{1,0:T(8,128)(2,1)S(1)} %convolution_add_fusion.15), channel_id=5, replica_groups=mesh['sp_0'=4,'sp_1'=4,'tp'=16] {'sp_0'}, dimensions={0}, use_global_device_ids=true | all-gather | bytes 163840 | tf_op jit(solution)/shard_map/all_gather | solution.py:26
  359.0 12.0 %all-gather.4 = bf16[4,128,128]{2,1,0:T(8,128)(2,1)S(1)} all-gather(bf16[1,128,128]{2,1,0:T(8,128)(2,1)S(1)} %get-tuple-element.236), channel_id=6, replica_groups=mesh['sp_0'=4,'sp_1'=4,'tp'=16] {'sp_1'}, dimensions={0}, use_global_device_ids=true | all-gather | bytes 163840 | tf_op jit(solution)/shard_map/all_gather | solution.py:26
  372.6 12.2 %all-gather.5 = bf16[512,128]{1,0:T(8,128)(2,1)S(1)} all-gather(bf16[128,128]{1,0:T(8,128)(2,1)S(1)} %fusion.229), channel_id=7, replica_groups=mesh['sp_0'=4,'sp_1'=4,'tp'=16] {'sp_0'}, dimensions={0}, use_global_device_ids=true | all-gather | bytes 163840 | tf_op jit(solution)/shard_map/all_gather | solution.py:26
  384.8 12.0 %all-gather.6 = bf16[4,128,128]{2,1,0:T(8,128)(2,1)S(1)} all-gather(bf16[1,128,128]{2,1,0:T(8,128)(2,1)S(1)} %get-tuple-element.237), channel_id=8, replica_groups=mesh['sp_0'=4,'sp_1'=4,'tp'=16] {'sp_1'}, dimensions={0}, use_global_device_ids=true | all-gather | bytes 163840 | tf_op jit(solution)/shard_map/all_gather | solution.py:26
  398.4 12.0 %all-gather.7 = bf16[512,128]{1,0:T(8,128)(2,1)S(1)} all-gather(bf16[128,128]{1,0:T(8,128)(2,1)S(1)} %convolution_add_fusion.6), channel_id=9, replica_groups=mesh['sp_0'=4,'sp_1'=4,'tp'=16] {'sp_0'}, dimensions={0}, use_global_device_ids=true | all-gather | bytes 163840 | tf_op jit(solution)/shard_map/all_gather | solution.py:26
  413.0 1.0 copy.130
  414.1 3.9 slice.185
  418.0 1.2 fusion.64
  419.2 2.0 convolution_bitcast_fusion.2
  421.2 1.7 fusion.68
  422.9 1.5 multiply_reduce_fusion.1
  424.5 1.1 copy.119
  425.6 4.4 convolution_convert_fusion.1
  431.1 1.3 gather_fusion.1
  432.6 61.9 %reduce-scatter.3.cloned.1.call-done = bf16[64,2048]{1,0:T(8,128)(2,1)} async-done(((bf16[1024,2048]{1,0:T(8,128)(2,1)}), bf16[64,2048]{1,0:T(8,128)(2,1)}) %reduce-scatter.3.cloned.1.call-update) | async-done | bytes 262160 | tf_op jit(solution)/shard_map/reduce_scatter | solution.py:173
  494.5 1.1 multiply_reduce_fusion
  495.7 1.3 fusion.37
  497.0 15.8 %all_to_all.15 = bf16[16,8,2048]{2,1,0:T(8,128)(2,1)S(1)} all-to-all(bf16[16,8,2048]{2,1,0:T(8,128)(2,1)S(1)} %fusion.37), channel_id=1, replica_groups=mesh['sp_0'=4,'sp_1'=4,'tp'=16] {'sp_0','sp_1'}, dimensions={0} | all-to-all | bytes 1048576 | tf_op jit(solution)/shard_map/all_to_all | solution.py:211
  512.8 1.1 stack.3
  513.9 189.6 %all_to_all.16 = bf16[16,128,2048]{2,1,0:T(8,128)(2,1)S(1)} all-to-all(bf16[16,128,2048]{2,1,0:T(8,128)(2,1)S(1)} %stack.3), channel_id=1, replica_groups=mesh['sp_0'=4,'sp_1'=4,'tp'=16] {'tp'}, dimensions={0} | all-to-all | bytes 16777216 | tf_op jit(solution)/shard_map/all_to_all | solution.py:216
  703.5 3.2 copy-done.1
  706.7 2.4 fusion.86
  709.2 12.9 %convolution_convert_fusion = bf16[2048,2048]{1,0:T(8,128)(2,1)} fusion(bf16[2048,2048]{1,0:T(8,128)(2,1)} %bitcast.418, f32[2048,128]{1,0:T(8,128)S(1)} %fusion.86, bf16[1,2048,128]{2,1,0:T(8,128)(2,1)S(1)} %copy-done, bf16[1,2048,128]{2,1,0:T(8,128)(2,1)S(1)} %copy-done.7), kind=kOutput, calls=%fused_computation.46 | convolution fusion | flops 2153250816 | bytes 18874368 | tf_op jit(solution)/shard_map/dot_general | solution.py:221
  722.8 65.8 %reduce-scatter.5.cloned.1.call-done = bf16[128,2048]{1,0:T(8,128)(2,1)} async-done(((bf16[2048,2048]{1,0:T(8,128)(2,1)}), bf16[128,2048]{1,0:T(8,128)(2,1)}) %reduce-scatter.5.cloned.1.call-update) | async-done | bytes 524304 | tf_op jit(solution)/shard_map/reduce_scatter | solution.py:224
  788.5 7.3 all-to-all-start.2
  796.3 8.3 %all-to-all-done.2 = bf16[16,8,2048]{2,1,0:T(8,128)(2,1)S(1)} async-done(((bf16[16,8,2048]{2,1,0:T(8,128)(2,1)}), bf16[16,8,2048]{2,1,0:T(8,128)(2,1)S(1)}, u32[]{:S(2)}, u32[]{:S(2)}) %all-to-all-start.2) | async-done | bytes 524320 | tf_op jit(solution)/shard_map/all_to_all | solution.py:231
  (366 shorter events, 119.9 us)
Async XLA Ops:
  6.5 702.6 %copy-start = (bf16[1,2048,128]{2,1,0:T(8,128)(2,1)S(1)}, bf16[1,2048,128]{2,1,0:T(8,128)(2,1)}, u32[]{:S(2)}) copy-start(bf16[1,2048,128]{2,1,0:T(8,128)(2,1)} %param.41) | copy-start | bytes 1572868
  6.5 488.0 %reduce-scatter.3.cloned.1.call-start = ((), (), s32[]{:S(2)}) async-start(), calls=%async_computation.5 | async-start | bytes 4456448 | tf_op jit(solution)/shard_map/reduce_scatter | solution.py:173
  7.8 83.5 %copy-start.23 = (bf16[1024,1,128]{2,0,1:T(8,128)(2,1)S(1)}, bf16[1024,1,128]{2,0,1:T(8,128)(2,1)}, u32[]{:S(2)}) copy-start(bf16[1024,1,128]{2,0,1:T(8,128)(2,1)} %param.26) | copy-start | bytes 786436
  8.8 82.5 %copy-start.42 = (f32[64,64]{1,0:T(8,128)}, f32[64,64]{1,0:T(8,128)S(1)}, u32[]{:S(2)}) copy-start(f32[64,64]{1,0:T(8,128)S(1)} %get-tuple-element.256) | copy-start | bytes 49156
  8.8 82.5 %copy-start.48 = (pred[64,64]{1,0:T(8,128)(4,1)}, pred[64,64]{1,0:T(8,128)(4,1)S(1)}, u32[]{:S(2)}) copy-start(pred[64,64]{1,0:T(8,128)(4,1)S(1)} %get-tuple-element.255) | copy-start | bytes 12292
  8.9 82.5 %copy-start.43 = (f32[64,64]{1,0:T(8,128)}, f32[64,64]{1,0:T(8,128)S(1)}, u32[]{:S(2)}) copy-start(f32[64,64]{1,0:T(8,128)S(1)} %fusion.185) | copy-start | bytes 49156
  11.3 80.0 %copy-start.50 = (pred[64,64]{1,0:T(8,128)(4,1)}, pred[64,64]{1,0:T(8,128)(4,1)S(1)}, u32[]{:S(2)}) copy-start(pred[64,64]{1,0:T(8,128)(4,1)S(1)} %get-tuple-element.253) | copy-start | bytes 12292
  11.8 79.6 %copy-start.52 = (f32[16]{0:T(128)}, f32[16]{0:T(128)S(1)}, u32[]{:S(2)}) copy-start(f32[16]{0:T(128)S(1)} %slice_reduce_fusion.1) | copy-start | bytes 196
  93.6 1.9 copy-start.5
  93.6 2.9 copy-start.4
  97.5 7.8 copy-start.49
  105.3 81.7 %copy-start.54 = (f32[16]{0:T(128)}, f32[16]{0:T(128)S(1)}, u32[]{:S(2)}) copy-start(f32[16]{0:T(128)S(1)} %slice_reduce_fusion) | copy-start | bytes 196
  192.3 0.6 copy-start.55
  246.9 1.0 copy-start.6
  249.2 0.8 copy-start.53
  319.3 0.6 copy-start.33
  320.0 12.8 %copy-start.24 = (bf16[128,128]{1,0:T(8,128)(2,1)}, bf16[128,128]{1,0:T(8,128)(2,1)S(1)}, u32[]{:S(2)}) copy-start(bf16[128,128]{1,0:T(8,128)(2,1)S(1)} %fusion.228) | copy-start | bytes 98308
  320.1 12.7 %copy-start.26 = (bf16[128,128]{1,0:T(8,128)(2,1)}, bf16[128,128]{1,0:T(8,128)(2,1)S(1)}, u32[]{:S(2)}) copy-start(bf16[128,128]{1,0:T(8,128)(2,1)S(1)} %fusion.227) | copy-start | bytes 98308
  320.3 12.5 %copy-start.28 = (bf16[128,128]{1,0:T(8,128)(2,1)}, bf16[128,128]{1,0:T(8,128)(2,1)S(1)}, u32[]{:S(2)}) copy-start(bf16[128,128]{1,0:T(8,128)(2,1)S(1)} %fusion.226) | copy-start | bytes 98308
  344.9 27.1 %copy-start.11 = (bf16[128,128]{1,0:T(8,128)(2,1)}, bf16[128,128]{1,0:T(8,128)(2,1)S(1)}, u32[]{:S(2)}) copy-start(bf16[128,128]{1,0:T(8,128)(2,1)S(1)} %convolution_add_fusion.18) | copy-start | bytes 98308
  345.1 0.6 copy-start.15
  345.8 26.2 %copy-start.17 = (bf16[128,128]{1,0:T(8,128)(2,1)}, bf16[128,128]{1,0:T(8,128)(2,1)S(1)}, u32[]{:S(2)}) copy-start(bf16[128,128]{1,0:T(8,128)(2,1)S(1)} %convolution_add_fusion.16) | copy-start | bytes 98308
  346.0 26.1 %copy-start.13 = (bf16[128,128]{1,0:T(8,128)(2,1)}, bf16[128,128]{1,0:T(8,128)(2,1)S(1)}, u32[]{:S(2)}) copy-start(bf16[128,128]{1,0:T(8,128)(2,1)S(1)} %convolution_add_fusion.15) | copy-start | bytes 98308
  358.0 52.7 %copy-start.8 = (bf16[512,128]{1,0:T(8,128)(2,1)}, bf16[512,128]{1,0:T(8,128)(2,1)S(1)}, u32[]{:S(2)}) copy-start(bf16[512,128]{1,0:T(8,128)(2,1)S(1)} %all-gather.3) | copy-start | bytes 393220
  358.1 0.9 copy-start.36
  358.2 0.8 copy-start.39
  371.2 0.6 copy-start.35
  371.9 0.6 copy-start.30
  372.5 12.3 %copy-start.31 = (bf16[128,128]{1,0:T(8,128)(2,1)}, bf16[128,128]{1,0:T(8,128)(2,1)S(1)}, u32[]{:S(2)}) copy-start(bf16[128,128]{1,0:T(8,128)(2,1)S(1)} %fusion.230) | copy-start | bytes 98308
  372.6 24.2 %copy-start.32 = (bf16[128,128]{1,0:T(8,128)(2,1)}, bf16[128,128]{1,0:T(8,128)(2,1)S(1)}, u32[]{:S(2)}) copy-start(bf16[128,128]{1,0:T(8,128)(2,1)S(1)} %fusion.229) | copy-start | bytes 98308
  384.8 27.9 %copy-start.9 = (bf16[512,128]{1,0:T(8,128)(2,1)}, bf16[512,128]{1,0:T(8,128)(2,1)S(1)}, u32[]{:S(2)}) copy-start(bf16[512,128]{1,0:T(8,128)(2,1)S(1)} %all-gather.5) | copy-start | bytes 393220
  396.9 0.6 copy-start.19
  397.1 0.6 copy-start.21
  397.7 0.6 copy-start.22
  398.4 12.3 %copy-start.20 = (bf16[128,128]{1,0:T(8,128)(2,1)}, bf16[128,128]{1,0:T(8,128)(2,1)S(1)}, u32[]{:S(2)}) copy-start(bf16[128,128]{1,0:T(8,128)(2,1)S(1)} %convolution_add_fusion.6) | copy-start | bytes 98308
  410.4 2.3 copy-start.10
  410.6 0.6 copy-start.38
  411.2 0.6 copy-start.41
  414.0 7.2 copy-start.25
  414.0 7.2 copy-start.27
  414.0 7.2 copy-start.29
  414.0 7.2 copy-start.34
  414.0 7.2 copy-start.37
  414.1 7.2 copy-start.40
  414.1 7.2 copy-start.44
  414.1 8.8 %copy-start.12 = (bf16[128,128]{1,0:T(8,128)(2,1)S(1)}, bf16[128,128]{1,0:T(8,128)(2,1)}, u32[]{:S(2)}) copy-start(bf16[128,128]{1,0:T(8,128)(2,1)} %copy-done.11) | copy-start | bytes 98308
  414.1 8.8 %copy-start.14 = (bf16[128,128]{1,0:T(8,128)(2,1)S(1)}, bf16[128,128]{1,0:T(8,128)(2,1)}, u32[]{:S(2)}) copy-start(bf16[128,128]{1,0:T(8,128)(2,1)} %copy-done.13) | copy-start | bytes 98308
  414.1 8.8 %copy-start.16 = (bf16[128,128]{1,0:T(8,128)(2,1)S(1)}, bf16[128,128]{1,0:T(8,128)(2,1)}, u32[]{:S(2)}) copy-start(bf16[128,128]{1,0:T(8,128)(2,1)} %copy-done.15) | copy-start | bytes 98308
  414.1 8.8 %copy-start.18 = (bf16[128,128]{1,0:T(8,128)(2,1)S(1)}, bf16[128,128]{1,0:T(8,128)(2,1)}, u32[]{:S(2)}) copy-start(bf16[128,128]{1,0:T(8,128)(2,1)} %copy-done.17) | copy-start | bytes 98308
  422.9 2.6 copy-start.51
  429.9 0.7 copy-start.46
  430.0 358.6 %reduce-scatter.5.cloned.1.call-start = ((), (), s32[]{:S(2)}) async-start(), calls=%async_computation.6 | async-start | bytes 8912896 | tf_op jit(solution)/shard_map/reduce_scatter | solution.py:224
  431.1 63.4 %copy-start.2 = (bf16[64,2048]{1,0:T(8,128)(2,1)S(1)}, bf16[64,2048]{1,0:T(8,128)(2,1)}, u32[]{:S(2)}) copy-start(bf16[64,2048]{1,0:T(8,128)(2,1)} %param.34) | copy-start | bytes 786436
  431.1 64.6 %copy-start.47 = (f32[2048]{0:T(1024)S(1)}, f32[2048]{0:T(1024)}, u32[]{:S(2)}) copy-start(f32[2048]{0:T(1024)} %param.35) | copy-start | bytes 24580
  513.9 192.9 %copy-start.57 = (bf16[1,2048,128]{2,1,0:T(8,128)(2,1)S(1)}, bf16[1,2048,128]{2,1,0:T(8,128)(2,1)}, u32[]{:S(2)}) copy-start(bf16[1,2048,128]{2,1,0:T(8,128)(2,1)} %param.39) | copy-start | bytes 1572868
  703.5 3.2 copy-start.1
  706.7 2.4 copy-start.7
  722.0 0.7 copy-start.45
  722.1 73.8 %copy-start.56 = (f32[64,2]{0,1:T(2,128)S(1)}, f32[64,2]{0,1:T(2,128)}, u32[]{:S(2)}) copy-start(f32[64,2]{0,1:T(2,128)} %param.37) | copy-start | bytes 1540
  788.5 16.1 %all-to-all-start.2 = ((bf16[16,8,2048]{2,1,0:T(8,128)(2,1)}), bf16[16,8,2048]{2,1,0:T(8,128)(2,1)S(1)}, u32[]{:S(2)}, u32[]{:S(2)}) async-start(bf16[16,8,2048]{2,1,0:T(8,128)(2,1)} %bitcast.438), calls=%async_computation.4 | async-start | bytes 1048576 | tf_op jit(solution)/shard_map/all_to_all | solution.py:231
  805.5 1.0 copy-start.3
Sparse Core Ops, SparseCore 0:
  430.1 64.3 reduce-scatter.2
  722.2 66.2 reduce-scatter.4
